TPU v7x, 32 devices: a whole 2x2x4 slice. The times are simulated.
32 devices in a mesh: grp: 2 (over x), ep: 16 (over z, y, core).
Axes of the slice: x: 2, y: 2, z: 4, core: 2. Of those that a mesh axis runs over, the one named last changes fastest.
Arguments:
- tokens: bfloat16 [256, 2048], P(('grp', 'ep')), parts along dimension 0, may hold values from -6 to 6
- first_gain: bfloat16 [2048], replicated, may hold values from 0.099609375 to 1.8984375
- query_weight: bfloat16 [2048, 1024], P(None, 'ep'), may hold values from -0.125 to 0.125
- key_weight: bfloat16 [2048, 1024], P(None, 'ep'), may hold values from -0.125 to 0.125
- value_weight: bfloat16 [2048, 1024], P(None, 'ep'), may hold values from -0.125 to 0.125
- outgate_weight: bfloat16 [2048, 1024], P(None, 'ep'), may hold values from -0.125 to 0.125
- igate_weight: bfloat16 [2048, 8], replicated, may hold values from -0.125 to 0.125
- fgate_weight: bfloat16 [2048, 8], replicated, may hold values from -0.125 to 0.125
- igate_bias: float32 [8], replicated, may hold values from -2 to 1
- fgate_bias: float32 [8], replicated, may hold values from -1 to 4
- memory_state: float32 [256, 8, 128, 128], P(('grp', 'ep')), parts along dimension 0, may hold values from -0.6 to 0.6
- norm_state: float32 [256, 8, 128], P(('grp', 'ep')), parts along dimension 0, may hold values from -0.6 to 0.6
- max_state: float32 [256, 8], P(('grp', 'ep')), parts along dimension 0, may hold values from -1 to 2
- head_gain: bfloat16 [1024], replicated, may hold values from 0.099609375 to 1.8984375
- out_weight: bfloat16 [1024, 2048], P('ep'), may hold values from -0.1875 to 0.1875
- second_gain: bfloat16 [2048], replicated, may hold values from 0.099609375 to 1.8984375
- expert_ids: int32 [256, 6], P(('grp', 'ep')), parts along dimension 0, may hold values from 0 to 15, all different within a row; in each aligned block of 8 rows (0 to 7, 8 to 15, ...) at most 6 rows name the same one
- route_weight: float32 [256, 6], P(('grp', 'ep')), parts along dimension 0, may hold values from 0.2 to 1
- expert_gate: bfloat16 [16, 2048, 256], P('ep'), may hold values from -0.125 to 0.125
- expert_up: bfloat16 [16, 2048, 256], P('ep'), may hold values from -0.125 to 0.125
- expert_down: bfloat16 [16, 256, 2048], P('ep'), may hold values from -0.375 to 0.375
- shared_gate: bfloat16 [2048, 256], P('ep'), may hold values from -0.125 to 0.125
- shared_up: bfloat16 [2048, 256], P('ep'), may hold values from -0.125 to 0.125
- shared_down: bfloat16 [256, 2048], P(None, 'ep'), may hold values from -0.375 to 0.375
Outputs:
- mixed_out: bfloat16 [256, 2048], P(('grp', 'ep')), parts along dimension 0
- memory_next: float32 [256, 8, 128, 128], P(('grp', 'ep')), parts along dimension 0
- norm_next: float32 [256, 8, 128], P(('grp', 'ep')), parts along dimension 0
- max_next: float32 [256, 8], P(('grp', 'ep')), parts along dimension 0
There are 2 independent parts, one for each index of `grp`. A program takes and returns all parts, laid end to end along the dimension named above; an argument that names none is the same for every part. Nothing has to cross between parts.
Inputs may be any that keep to these rules, and one draw needn't show every extreme that they name: `expert_ids`: each row names 6 different experts. Among the rows of one device no expert is named by more than 6 rows, and in every draw some expert is named by exactly 6 rows of some device.
All inputs are finite; a program needn't handle non-finite values.
Results may differ from a plain program's by a relative error of at most 0.013.
Values may be sent and summed in bfloat16 or wider, within the bound.
A program may use at most 64 MiB of HBM per device.

v0:
```python
import jax
import jax.numpy as jnp
from jax import lax
from jax.experimental import pallas as pl
from jax.experimental.pallas import tpu as pltpu
from jax.sharding import PartitionSpec as P
import functools

epsilon = 1e-06


def rms_scale(values, gain):
    return (
        values
        * lax.rsqrt(jnp.mean(values * values, axis=-1, keepdims=True) + epsilon)
        * gain.astype(jnp.float32)
    )


def cell_step(
    normed,
    query,
    key_proj,
    value_proj,
    outgate,
    igate_weight,
    fgate_weight,
    igate_bias,
    fgate_bias,
    memory_state,
    norm_state,
    max_state,
    head_gain,
):
    row_count, head_count = max_state.shape
    head_size = memory_state.shape[-1]
    input_gate = jnp.dot(normed, igate_weight, preferred_element_type=jnp.float32) + igate_bias
    forget_log = jax.nn.log_sigmoid(
        jnp.dot(normed, fgate_weight, preferred_element_type=jnp.float32) + fgate_bias
    )
    query_heads = query.astype(jnp.float32).reshape(row_count, head_count, head_size)
    key_heads = key_proj.astype(jnp.float32).reshape(
        row_count, head_count, head_size
    ) * head_size ** (-0.5)
    value_heads = value_proj.astype(jnp.float32).reshape(row_count, head_count, head_size)
    max_next = jnp.maximum(forget_log + max_state, input_gate)
    decay_rate = jnp.exp(forget_log + max_state - max_next)
    injected = jnp.exp(input_gate - max_next)
    memory_next = decay_rate[:, :, None, None] * memory_state + injected[:, :, None, None] * (
        key_heads[:, :, :, None] * value_heads[:, :, None, :]
    )
    norm_next = decay_rate[:, :, None] * norm_state + injected[:, :, None] * key_heads
    numerator = jnp.einsum(
        "shd,shde->she", query_heads, memory_next, precision=lax.Precision.HIGHEST
    )
    denominator = jnp.maximum(
        jnp.abs(jnp.sum(query_heads * norm_next, axis=-1)), jnp.exp(-max_next)
    )
    readout = numerator / denominator[:, :, None]
    readout = rms_scale(readout, head_gain.reshape(head_count, head_size))
    gated = readout.reshape(row_count, head_count * head_size) * jax.nn.sigmoid(
        outgate.astype(jnp.float32)
    )
    return (gated.astype(jnp.bfloat16), memory_next, norm_next, max_next)


def shards(
    tokens,
    first_gain,
    query_weight,
    key_weight,
    value_weight,
    outgate_weight,
    igate_weight,
    fgate_weight,
    igate_bias,
    fgate_bias,
    memory_state,
    norm_state,
    max_state,
    head_gain,
    out_weight,
    second_gain,
    expert_ids,
    route_weight,
    expert_gate,
    expert_up,
    expert_down,
    shared_gate,
    shared_up,
    shared_down,
):
    own_rows = tokens.shape[0]
    devices = lax.axis_size("ep")
    top_count = expert_ids.shape[1]
    capacity = max(2, 2 * own_rows * top_count // devices)
    inputs = tokens.astype(jnp.float32)
    normed = rms_scale(inputs, first_gain).astype(jnp.bfloat16)
    block_rows = lax.all_gather(normed, "ep", axis=0, tiled=True)
    columns = jnp.stack(
        [
            jnp.dot(block_rows, matrix, preferred_element_type=jnp.float32).astype(jnp.bfloat16)
            for matrix in (query_weight, key_weight, value_weight, outgate_weight)
        ]
    )
    projected = lax.all_to_all(columns, "ep", split_axis=1, concat_axis=2, tiled=True)
    gated, memory_next, norm_next, max_next = cell_step(
        normed,
        projected[0],
        projected[1],
        projected[2],
        projected[3],
        igate_weight,
        fgate_weight,
        igate_bias,
        fgate_bias,
        memory_state,
        norm_state,
        max_state,
        head_gain,
    )
    picked = gated
    mix_sums = jnp.dot(
        picked,
        lax.all_gather(out_weight, "ep", axis=0, tiled=True),
        preferred_element_type=jnp.float32,
    )
    stream = inputs + mix_sums.astype(jnp.bfloat16).astype(jnp.float32)
    normed_two = rms_scale(stream, second_gain).astype(jnp.bfloat16)
    block_rows = (
        lax.all_gather(shared_gate, "ep", axis=0, tiled=True),
        lax.all_gather(shared_up, "ep", axis=0, tiled=True),
    )
    picked = normed_two
    gate_shared = jnp.dot(picked, block_rows[0], preferred_element_type=jnp.float32)
    up_shared = jnp.dot(picked, block_rows[1], preferred_element_type=jnp.float32)
    hidden_shared = (jax.nn.silu(gate_shared) * up_shared).astype(jnp.bfloat16)
    shared_result = jnp.dot(
        hidden_shared,
        lax.all_gather(shared_down, "ep", axis=1, tiled=True),
        preferred_element_type=jnp.float32,
    )
    choose = (expert_ids[:, :, None] == jnp.arange(devices, dtype=jnp.int32)[None, None, :]).astype(
        jnp.int32
    )
    counted = jnp.sum(choose, axis=1)
    ranking = jnp.cumsum(counted, axis=0) - counted
    slot_index = jnp.sum(choose * ranking[:, None, :], axis=2)
    slot_ids = jnp.arange(capacity, dtype=jnp.int32)
    selector = counted.T[:, None, :] * (ranking.T[:, None, :] == slot_ids[None, :, None]).astype(
        jnp.int32
    )
    outgoing = jnp.einsum(
        "ecr,rd->ecd", selector.astype(jnp.bfloat16), normed_two, preferred_element_type=jnp.float32
    ).astype(jnp.bfloat16)
    arrived = lax.all_to_all(outgoing, "ep", split_axis=0, concat_axis=0, tiled=True)
    sources, slots, width = arrived.shape
    flat_rows = arrived.reshape(sources * slots, width)
    gate_sums = jnp.dot(flat_rows, expert_gate[0], preferred_element_type=jnp.float32)
    up_sums = jnp.dot(flat_rows, expert_up[0], preferred_element_type=jnp.float32)
    hidden = (jax.nn.silu(gate_sums) * up_sums).astype(jnp.bfloat16)
    result = jnp.dot(hidden, expert_down[0], preferred_element_type=jnp.float32).astype(
        jnp.bfloat16
    )
    results = lax.all_to_all(
        result.reshape(sources, slots, width), "ep", split_axis=0, concat_axis=0, tiled=True
    )
    flat_results = results.reshape(devices * capacity, results.shape[2])
    picked_results = flat_results[expert_ids * capacity + slot_index]
    routed = jnp.sum(route_weight[:, :, None] * picked_results.astype(jnp.float32), axis=1)
    mixed_out = (stream + routed + shared_result).astype(jnp.bfloat16)
    return (mixed_out, memory_next, norm_next, max_next)


ANY, VMEM = pl.ANY, pltpu.VMEM
F32, BF16 = jnp.float32, jnp.bfloat16


def remote(source, target, send, receive, device):
    return pltpu.make_async_remote_copy(
        src_ref=source,
        dst_ref=target,
        send_sem=send,
        recv_sem=receive,
        device_id={"ep": device},
        device_id_type=pl.DeviceIdType.MESH,
    )


def across(left, right):
    return lax.dot_general(left, right, (((1,), (1,)), ((), ())), preferred_element_type=F32)


def in_line(gain):
    held = gain[...].astype(F32)
    return jnp.concatenate([held[i : i + 1] for i in range(held.shape[0])], axis=1)


def fused(
    n,
    tokens,
    first_gain,
    query_weight,
    key_weight,
    value_weight,
    outgate_weight,
    igate_weight,
    fgate_weight,
    igate_bias,
    fgate_bias,
    memory_state,
    norm_state,
    max_state,
    head_gain,
    out_weight,
    second_gain,
    expert_ids,
    route_weight,
    expert_gate,
    expert_up,
    expert_down,
    shared_gate,
    shared_up,
    shared_down,
    mixed_out,
    memory_next,
    norm_next,
    max_next,
    proj,
    gates_in,
    memory,
    out_pad,
    wide,
    down,
    rows_one,
    rows_two,
    table,
    column_send,
    column_recv,
    shared_send,
    shared_recv,
    sdown_recv,
    gated_send,
    gated_recv,
    part,
    part_send,
    pair_recv,
    sum_send,
    sum_recv,
    local_sem,
    memory_in_sem,
    send_sem,
    recv_sem,
    gather_sem,
    pair_sem,
    sum_sem,
):
    rows, width = tokens.shape
    heads, size = memory_state.shape[1], memory_state.shape[3]
    cut = query_weight.shape[0]
    share = size // cut
    hidden = shared_gate.shape[1] // n
    top_count = expert_ids.shape[1]
    chips = n // 2
    me = lax.axis_index("ep")
    side, chip = me % 2, me // 2
    partner = me + 1 - 2 * side

    barrier = pltpu.get_barrier_semaphore()
    for k in range(1, n):
        pl.semaphore_signal(
            barrier,
            inc=1,
            device_id={"ep": (me + k) % n},
            device_id_type=pl.DeviceIdType.MESH,
        )

    loads = []

    def load(source, target):
        copy = pltpu.make_async_copy(source, target, local_sem.at[len(loads)])
        copy.start()
        loads.append(copy)
        return copy

    proj_loads = [
        load(matrix, proj.at[pl.ds(i * cut, cut)])
        for i, matrix in enumerate((query_weight, key_weight, value_weight, outgate_weight))
    ]
    gate_loads = [load(igate_weight, gates_in.at[0]), load(fgate_weight, gates_in.at[1])]
    memory_loads = []
    for h in range(heads):
        copy = pltpu.make_async_copy(
            memory_state.at[:, h], memory.at[:, h], memory_in_sem.at[h]
        )
        copy.start()
        memory_loads.append(copy)
    spot = pl.multiple_of((me % share) * cut, cut)
    out_load = load(out_weight, out_pad.at[pl.ds(spot, cut)])
    wide_loads = [load(expert_gate.at[0], wide.at[0]), load(expert_up.at[0], wide.at[1])]
    down_load = load(expert_down.at[0], down)

    inputs = tokens[...].astype(F32)
    rows_one[me] = rms_scale(inputs, in_line(first_gain)).astype(BF16)

    pl.semaphore_wait(barrier, n - 1)

    def gather(buffer, which):
        sends = []
        for k in range(chips - 1, 0, -1):
            there = 2 * ((chip + k) % chips) + side
            sends.append(
                remote(
                    buffer.at[me],
                    buffer.at[me],
                    gather_sem.at[which, 0, k],
                    gather_sem.at[which, 1, k],
                    there,
                )
            )
            sends[-1].start()
        near = remote(
            buffer.at[me],
            buffer.at[me],
            gather_sem.at[which, 2, 0],
            gather_sem.at[which, 3, 0],
            partner,
        )
        near.start()
        return sends, near

    def gather_end(buffer, which, sends, near):
        passed = [near]
        for k in ORDER(chips):
            slot = 2 * ((chip + chips - k) % chips) + side
            sends[chips - 1 - k].wait_recv()
            onward = remote(
                buffer.at[slot],
                buffer.at[slot],
                gather_sem.at[which, 2, k],
                gather_sem.at[which, 3, k],
                partner,
            )
            onward.start()
            passed.append(onward)
        for copy in passed:
            copy.wait_recv()
        return sends + passed

    unsent = []
    first = gather(rows_one, 0)

    for i in range(1, share):
        other = pl.multiple_of(((me + i) % share) * cut, cut)
        out_pad[pl.ds(other, cut), :] = jnp.zeros((cut, width), BF16)
    lanes = lax.broadcasted_iota(jnp.int32, (rows, 128), 1)
    routes = jnp.zeros((rows, 128), F32)
    for t in range(top_count):
        routes = routes + jnp.where(
            expert_ids[:, t : t + 1] == lanes, route_weight[:, t : t + 1], 0.0
        )
    table[me] = routes
    for i, matrix in enumerate((shared_gate, shared_up)):
        turned = matrix[...].astype(F32).T.reshape(n, hidden, matrix.shape[0])
        shared_send[:, i * hidden : (i + 1) * hidden, :] = turned.astype(BF16)
    for copy in gate_loads:
        copy.wait()
    own = rows_one[me]
    input_gate = across(own, gates_in[0]) + igate_bias[...]
    forget_log = jax.nn.log_sigmoid(across(own, gates_in[1]) + fgate_bias[...])
    kept = forget_log + max_state[...]
    top = jnp.maximum(kept, input_gate)
    max_next[...] = top
    decay_rate = jnp.exp(kept - top)
    injected = jnp.exp(input_gate - top)
    floor = jnp.exp(-top)

    unsent += gather_end(rows_one, 0, *first)

    def flat(buffer):
        held = buffer[...].astype(F32)
        return held.reshape(n * rows, held.shape[2])

    for copy in proj_loads:
        copy.wait()
    columns = across(flat(rows_one).astype(BF16), proj[...])
    column_send[...] = columns.reshape(n, rows, 4 * cut).astype(BF16)

    def spread(which, source, target):
        for k in range(1, n):
            there = (me + k) % n
            copy = remote(
                source(there), target, send_sem.at[which, k], recv_sem.at[which, k], there
            )
            copy.start()
            unsent.append(copy)

    def arrive(which, source, target):
        for k in range(1, n):
            remote(
                source(me), target, send_sem.at[which, k], recv_sem.at[which, k], (me + k) % n
            ).wait_recv()

    spread(0, lambda j: column_send.at[j], column_recv.at[me])
    column_recv[me] = column_send[me]
    spread(1, lambda j: table.at[me], table.at[me])
    arrive(0, lambda j: column_send.at[j], column_recv.at[me])
    spread(2, lambda j: shared_send.at[j], shared_recv.at[me])
    shared_recv[me] = shared_send[me]
    spread(3, lambda j: shared_down.at[j], sdown_recv.at[me])
    sdown_recv[me] = shared_down[me]

    for h in range(heads):
        pieces = [column_recv[h * share + i].astype(F32) for i in range(share)]
        query, keyed, valued, outgate = [
            jnp.concatenate([piece[:, i * cut : (i + 1) * cut] for piece in pieces], axis=1)
            for i in range(4)
        ]
        decay = jnp.broadcast_to(decay_rate[:, h : h + 1], (rows, size))
        inject = keyed * size ** (-0.5) * injected[:, h : h + 1]
        norm = decay * norm_state[:, h, :] + inject
        norm_next[:, h, :] = norm
        bottom = jnp.maximum(
            jnp.abs(jnp.sum(query * norm, axis=-1, keepdims=True)), floor[:, h : h + 1]
        )
        key_columns, query_columns = inject.T, query.T
        memory_loads[h].wait()
        tops = []
        for s in range(rows):
            cell = (
                decay[s : s + 1, :] * memory[s, h]
                + key_columns[:, s : s + 1] * valued[s : s + 1, :]
            )
            memory_next[s, h] = cell
            tops.append(jnp.sum(query_columns[:, s : s + 1] * cell, axis=0, keepdims=True))
        readout = jnp.concatenate(tops, axis=0) / bottom
        readout = rms_scale(readout, head_gain[h : h + 1, :])
        gated_send[h] = (readout * jax.nn.sigmoid(outgate)).astype(BF16)

    spread(4, lambda j: gated_send.at[j // share], gated_recv.at[me])
    gated_recv[me] = gated_send[me // share]
    out_load.wait()
    arrive(4, lambda j: gated_send.at[j // share], gated_recv.at[me])

    def scatter(which, total, value):
        part[...] = value.reshape(n, rows, width)
        pair = []
        for k in list(range(1, chips)) + [0]:
            c = (chip + k) % chips
            part_send[which, c] = part[2 * c + 1 - side].astype(BF16)
            copy = remote(
                part_send.at[which, c],
                pair_recv.at[which, c],
                pair_sem.at[which, 0, k],
                pair_sem.at[which, 1, k],
                partner,
            )
            copy.start()
            pair.append((k, c, copy))
        sends = []
        for k, c, copy in pair:
            copy.wait_recv()
            both = part[2 * c + side] + pair_recv[which, c].astype(F32)
            if k == 0:
                total = total + both if total is not None else both
                continue
            sum_send[which, c] = both.astype(BF16)
            away = remote(
                sum_send.at[which, c],
                sum_recv.at[which, chip],
                sum_sem.at[which, 0, k],
                sum_sem.at[which, 1, k],
                2 * c + side,
            )
            away.start()
            sends.append((k, away))
        for k, away in sends:
            away.wait_recv()
            total = total + sum_recv[which, (chip + chips - k) % chips].astype(F32)
        unsent.extend([copy for _, _, copy in pair] + [away for _, away in sends])
        return total

    mix = scatter(
        0, None, jnp.dot(flat(gated_recv).astype(BF16), out_pad[...], preferred_element_type=F32)
    )
    stream = tokens[...].astype(F32) + mix.astype(BF16).astype(F32)
    rows_two[me] = rms_scale(stream, in_line(second_gain)).astype(BF16)
    second = gather(rows_two, 1)
    for copy in wide_loads + [down_load]:
        copy.wait()
    arrive(1, lambda j: table.at[me], table.at[me])
    arrive(2, lambda j: shared_send.at[j], shared_recv.at[me])
    arrive(3, lambda j: shared_down.at[j], sdown_recv.at[me])
    weights = flat(table)
    mine = lax.broadcasted_iota(jnp.int32, weights.shape, 1) == me
    weight = jnp.sum(jnp.where(mine, weights, 0.0), axis=1, keepdims=True)
    shared_wide = jnp.concatenate([shared_recv[i] for i in range(n)], axis=1)
    shared_rows = jnp.concatenate([sdown_recv[i] for i in range(n)], axis=1)
    unsent += gather_end(rows_two, 1, *second)

    block = flat(rows_two).astype(BF16)
    gate_sums = jnp.dot(block, wide[0], preferred_element_type=F32)
    up_sums = jnp.dot(block, wide[1], preferred_element_type=F32)
    own_hidden = (jax.nn.silu(gate_sums) * up_sums).astype(BF16)
    both = across(block, shared_wide)
    shared_hidden = (jax.nn.silu(both[:, :hidden]) * both[:, hidden:]).astype(BF16)
    value = weight * jnp.dot(own_hidden, down[...], preferred_element_type=F32) + jnp.dot(
        shared_hidden, shared_rows, preferred_element_type=F32
    )
    mixed_out[...] = scatter(1, stream, value).astype(BF16)

    for copy in unsent:
        copy.wait_send()


def ORDER(chips):
    return range(chips - 1, 0, -1)


def fused_shards(n, *args):
    (tokens, first_gain, query_weight, key_weight, value_weight, outgate_weight, igate_weight,
     fgate_weight, igate_bias, fgate_bias, memory_state, norm_state, max_state, head_gain,
     out_weight, second_gain, expert_ids, route_weight, expert_gate, expert_up, expert_down,
     shared_gate, shared_up, shared_down) = args
    rows, width = tokens.shape
    heads, size = memory_state.shape[1], memory_state.shape[3]
    cut = query_weight.shape[1]
    hidden = shared_gate.shape[1] // n
    chips = n // 2
    inner = expert_gate.shape[2]
    operands = (
        tokens, first_gain.reshape(-1, 128), query_weight.T, key_weight.T, value_weight.T,
        outgate_weight.T, igate_weight.T, fgate_weight.T, igate_bias.reshape(1, -1), fgate_bias.reshape(1, -1),
        memory_state, norm_state, max_state, head_gain.reshape(heads, size), out_weight,
        second_gain.reshape(-1, 128), expert_ids, route_weight, expert_gate, expert_up, expert_down,
        shared_gate, shared_up, shared_down.reshape(n, hidden, shared_down.shape[1]),
    )
    far = {2, 3, 4, 5, 6, 7, 10, 14, 18, 19, 20}
    operands = [
        pltpu.with_memory_space_constraint(x, pltpu.HBM)
        for i, x in enumerate(operands)
    ]
    dma = pltpu.SemaphoreType.DMA
    return pl.pallas_call(
        functools.partial(fused, n),
        out_shape=(
            jax.ShapeDtypeStruct((rows, width), BF16),
            jax.ShapeDtypeStruct(memory_state.shape, F32),
            jax.ShapeDtypeStruct(norm_state.shape, F32),
            jax.ShapeDtypeStruct(max_state.shape, F32),
        ),
        in_specs=[
            pl.BlockSpec(memory_space=pltpu.HBM if i in far else VMEM) for i in range(len(operands))
        ],
        out_specs=tuple(pl.BlockSpec(memory_space=m) for m in (VMEM, VMEM, VMEM, VMEM)),
        scratch_shapes=[
            VMEM((4 * cut, width), BF16),
            VMEM((2, heads, width), BF16),
            VMEM(memory_state.shape, F32),
            VMEM((size, width), BF16),
            VMEM((2, width, inner), BF16),
            VMEM((inner, width), BF16),
            VMEM((n, rows, width), BF16),
            VMEM((n, rows, width), BF16),
            VMEM((n, rows, 128), F32),
            VMEM((n, rows, 4 * cut), BF16),
            VMEM((n, rows, 4 * cut), BF16),
            VMEM((n, 2 * hidden, shared_gate.shape[0]), BF16),
            VMEM((n, 2 * hidden, shared_gate.shape[0]), BF16),
            VMEM((n, hidden, shared_down.shape[1]), BF16),
            VMEM((heads, rows, size), BF16),
            VMEM((n, rows, size), BF16),
            VMEM((n, rows, width), F32),
            VMEM((2, chips, rows, width), BF16),
            VMEM((2, chips, rows, width), BF16),
            VMEM((2, chips, rows, width), BF16),
            VMEM((2, chips, rows, width), BF16),
            dma((10,)),
            dma((heads,)),
            dma((5, n)),
            dma((5, n)),
            dma((2, 4, chips)),
            dma((2, 2, chips)),
            dma((2, 2, chips)),
        ],
        compiler_params=pltpu.CompilerParams(
            collective_id=0, has_side_effects=True, vmem_limit_bytes=28 * 1024 * 1024
        ),
    )(*operands)


def fits(n, width, size, cut, hidden_all, experts, rows):
    return (
        n % 2 == 0
        and n <= 128
        and experts == n
        and width % (128 * n) == 0
        and hidden_all % (16 * n) == 0
        and size == 128
        and size % cut == 0
        and cut % 16 == 0
        and rows == 8
    )


def pick(n, *args):
    tokens, query_weight, memory_state = args[0], args[2], args[10]
    experts, hidden_all = args[18].shape[0] * n, args[21].shape[1]
    if fits(
        n, tokens.shape[1], memory_state.shape[3], query_weight.shape[1], hidden_all, experts,
        tokens.shape[0],
    ):
        return fused_shards(n, *args)
    return shards(*args)


def solution(mesh):
    placed = (
        P(("grp", "ep"), None),
        P(),
        P(None, "ep"),
        P(None, "ep"),
        P(None, "ep"),
        P(None, "ep"),
        P(),
        P(),
        P(),
        P(),
        P(("grp", "ep"), None, None, None),
        P(("grp", "ep"), None, None),
        P(("grp", "ep"), None),
        P(),
        P("ep", None),
        P(),
        P(("grp", "ep"), None),
        P(("grp", "ep"), None),
        P("ep", None, None),
        P("ep", None, None),
        P("ep", None, None),
        P("ep", None),
        P("ep", None),
        P(None, "ep"),
    )
    return jax.shard_map(
        functools.partial(pick, mesh.shape["ep"]),
        mesh=mesh,
        in_specs=placed,
        out_specs=(
            P(("grp", "ep"), None),
            P(("grp", "ep"), None, None, None),
            P(("grp", "ep"), None, None),
            P(("grp", "ep"), None),
        ),
        check_vma=False,
    )
```

profile of v0, /device:TPU:0, one launch (start us, length us, event | category | flops | bytes accessed | tf_op | source)
XLA Modules:
  0.0 61.6 jit_solution(16236311474885947285)
XLA Ops:
  0.6 57.2 %shard_map.255 = (bf16[8,2048]{1,0:T(8,128)(2,1)S(1)}, f32[8,8,128,128]{3,2,1,0:T(8,128)S(1)}, f32[8,8,128]{2,1,0:T(8,128)S(1)}, f32[8,8]{1,0:T(8,128)S(1)}) custom-call(bf16[8,2048]{1,0:T(8,128)(2,1)} %tokens.1, bf16[16,128]{1,0:T(8,128)(2,1)} %bitcast.19, bf16[64,2048]{1,0:T(8,128)(2,1)} %bitcast.12, bf16[64,2048]{1,0:T(8,128)(2,1)} %bitcast.13, ...), custom_call_target="tpu_custom_call" | custom-call | tf_op jit(solution)/shard_map/pallas_call | solution.py:544
  57.8 0.6 %copy.32 = bf16[8,2048]{1,0:T(8,128)(2,1)} copy(bf16[8,2048]{1,0:T(8,128)(2,1)S(1)} %get-tuple-element.8) | data formatting | bytes 65536
  58.4 2.0 %copy.33 = f32[8,8,128,128]{3,2,1,0:T(8,128)} copy(f32[8,8,128,128]{3,2,1,0:T(8,128)S(1)} %get-tuple-element.9) | data formatting | bytes 8388608
  60.4 0.6 copy.34
  61.0 0.6 copy.35
where the time goes:
time: 61.8 us; the launch traced here: 61.6 us
  Pallas kernels  57.2 us (93%)
  local copies, waits for them, and re-layouts  3.84 us (6%)
  between operations  0.65 us (1%)
    pallas_call x1, Pallas kernels, fused_shards(): pl.pallas_call(functools.partial(fused, n), out_shape=(jax.ShapeDtypeStru...  57.2 us
    unnamed x4, local copies, waits for them, and re-layouts  3.84 us

commit v1 on v0

--- a/solution.py
+++ b/solution.py
@@ -410,29 +410,49 @@
     spread(3, lambda j: shared_down.at[j], sdown_recv.at[me])
     sdown_recv[me] = shared_down[me]
 
+    place = lax.broadcasted_iota(jnp.int32, (rows, rows * size), 1) // size
+    diagonal = place == lax.broadcasted_iota(jnp.int32, (rows, rows * size), 0)
+    ones = jnp.where(diagonal, 1.0, 0.0)
+    blocks = jnp.concatenate([ones, jnp.zeros_like(ones)], axis=0)
+
+    def turned_dot(left, right):
+        return lax.dot_general(
+            left.astype(BF16),
+            right.astype(BF16),
+            (((0,), (0,)), ((), ())),
+            preferred_element_type=F32,
+        )
+
     for h in range(heads):
         pieces = [column_recv[h * share + i].astype(F32) for i in range(share)]
         query, keyed, valued, outgate = [
             jnp.concatenate([piece[:, i * cut : (i + 1) * cut] for piece in pieces], axis=1)
             for i in range(4)
         ]
+        scale = injected[:, h : h + 1] * size ** (-0.5)
         decay = jnp.broadcast_to(decay_rate[:, h : h + 1], (rows, size))
-        inject = keyed * size ** (-0.5) * injected[:, h : h + 1]
-        norm = decay * norm_state[:, h, :] + inject
+        norm = decay * norm_state[:, h, :] + scale * keyed
         norm_next[:, h, :] = norm
         bottom = jnp.maximum(
             jnp.abs(jnp.sum(query * norm, axis=-1, keepdims=True)), floor[:, h : h + 1]
         )
-        key_columns, query_columns = inject.T, query.T
+        spread_value = jnp.where(diagonal, jnp.concatenate([scale * valued] * rows, axis=1), 0.0)
+        high = spread_value.astype(BF16).astype(F32)
+        outer = turned_dot(
+            jnp.concatenate([keyed, keyed], axis=0),
+            jnp.concatenate([high, spread_value - high], axis=0),
+        )
+        wide_query = turned_dot(jnp.concatenate([query, query * 0.0], axis=0), blocks)
         memory_loads[h].wait()
         tops = []
         for s in range(rows):
-            cell = (
-                decay[s : s + 1, :] * memory[s, h]
-                + key_columns[:, s : s + 1] * valued[s : s + 1, :]
+            cell = decay[s : s + 1, :] * memory[s, h] + outer[:, s * size : (s + 1) * size]
+            memory_next[s, h] = cell
+            tops.append(
+                jnp.sum(
+                    wide_query[:, s * size : (s + 1) * size] * cell, axis=0, keepdims=True
+                )
             )
-            memory_next[s, h] = cell
-            tops.append(jnp.sum(query_columns[:, s : s + 1] * cell, axis=0, keepdims=True))
         readout = jnp.concatenate(tops, axis=0) / bottom
         readout = rms_scale(readout, head_gain[h : h + 1, :])
         gated_send[h] = (readout * jax.nn.sigmoid(outgate)).astype(BF16)

time: 61.8 us -> 60.8 us (0.984)
  Pallas kernels: 57.2 us -> 56.1 us
    pallas_call x1, Pallas kernels: 57.2 us -> 56.1 us  [fused_shards(): pl.pallas_call(functools.partial(fused, n), out_shape=(jax.ShapeDtypeStru...]
where the time goes in v1:
time: 60.8 us; the launch traced here: 60.6 us
  Pallas kernels  56.1 us (92%)
  local copies, waits for them, and re-layouts  3.84 us (6%)
  between operations  0.65 us (1%)
    pallas_call x1, Pallas kernels, fused_shards(): pl.pallas_call(functools.partial(fused, n), out_shape=(jax.ShapeDtypeStru...  56.1 us
    unnamed x4, local copies, waits for them, and re-layouts  3.84 us

profile of v1, /device:TPU:0, one launch (start us, length us, event | category | flops | bytes accessed | tf_op | source)
XLA Modules:
  0.0 60.6 jit_solution(897247891484516531)
XLA Ops:
  0.6 56.1 %shard_map.255 = (bf16[8,2048]{1,0:T(8,128)(2,1)S(1)}, f32[8,8,128,128]{3,2,1,0:T(8,128)S(1)}, f32[8,8,128]{2,1,0:T(8,128)S(1)}, f32[8,8]{1,0:T(8,128)S(1)}) custom-call(bf16[8,2048]{1,0:T(8,128)(2,1)} %tokens.1, bf16[16,128]{1,0:T(8,128)(2,1)} %bitcast.19, bf16[64,2048]{1,0:T(8,128)(2,1)} %bitcast.12, bf16[64,2048]{1,0:T(8,128)(2,1)} %bitcast.13, ...), custom_call_target="tpu_custom_call" | custom-call | tf_op jit(solution)/shard_map/pallas_call | solution.py:564
  56.8 0.6 %copy.32 = bf16[8,2048]{1,0:T(8,128)(2,1)} copy(bf16[8,2048]{1,0:T(8,128)(2,1)S(1)} %get-tuple-element.8) | data formatting | bytes 65536
  57.4 2.0 %copy.33 = f32[8,8,128,128]{3,2,1,0:T(8,128)} copy(f32[8,8,128,128]{3,2,1,0:T(8,128)S(1)} %get-tuple-element.9) | data formatting | bytes 8388608
  59.4 0.6 %copy.34 = f32[8,8,128]{2,1,0:T(8,128)} copy(f32[8,8,128]{2,1,0:T(8,128)S(1)} %get-tuple-element.10) | data formatting | bytes 65536
  60.0 0.6 copy.35

commit v2 on v1

v2 whole, which is shorter than its diff:
```python
import jax
import jax.numpy as jnp
from jax import lax
from jax.experimental import pallas as pl
from jax.experimental.pallas import tpu as pltpu
from jax.sharding import PartitionSpec as P
import functools

epsilon = 1e-06


def rms_scale(values, gain):
    return (
        values
        * lax.rsqrt(jnp.mean(values * values, axis=-1, keepdims=True) + epsilon)
        * gain.astype(jnp.float32)
    )


def cell_step(
    normed,
    query,
    key_proj,
    value_proj,
    outgate,
    igate_weight,
    fgate_weight,
    igate_bias,
    fgate_bias,
    memory_state,
    norm_state,
    max_state,
    head_gain,
):
    row_count, head_count = max_state.shape
    head_size = memory_state.shape[-1]
    input_gate = jnp.dot(normed, igate_weight, preferred_element_type=jnp.float32) + igate_bias
    forget_log = jax.nn.log_sigmoid(
        jnp.dot(normed, fgate_weight, preferred_element_type=jnp.float32) + fgate_bias
    )
    query_heads = query.astype(jnp.float32).reshape(row_count, head_count, head_size)
    key_heads = key_proj.astype(jnp.float32).reshape(
        row_count, head_count, head_size
    ) * head_size ** (-0.5)
    value_heads = value_proj.astype(jnp.float32).reshape(row_count, head_count, head_size)
    max_next = jnp.maximum(forget_log + max_state, input_gate)
    decay_rate = jnp.exp(forget_log + max_state - max_next)
    injected = jnp.exp(input_gate - max_next)
    memory_next = decay_rate[:, :, None, None] * memory_state + injected[:, :, None, None] * (
        key_heads[:, :, :, None] * value_heads[:, :, None, :]
    )
    norm_next = decay_rate[:, :, None] * norm_state + injected[:, :, None] * key_heads
    numerator = jnp.einsum(
        "shd,shde->she", query_heads, memory_next, precision=lax.Precision.HIGHEST
    )
    denominator = jnp.maximum(
        jnp.abs(jnp.sum(query_heads * norm_next, axis=-1)), jnp.exp(-max_next)
    )
    readout = numerator / denominator[:, :, None]
    readout = rms_scale(readout, head_gain.reshape(head_count, head_size))
    gated = readout.reshape(row_count, head_count * head_size) * jax.nn.sigmoid(
        outgate.astype(jnp.float32)
    )
    return (gated.astype(jnp.bfloat16), memory_next, norm_next, max_next)


def shards(
    tokens,
    first_gain,
    query_weight,
    key_weight,
    value_weight,
    outgate_weight,
    igate_weight,
    fgate_weight,
    igate_bias,
    fgate_bias,
    memory_state,
    norm_state,
    max_state,
    head_gain,
    out_weight,
    second_gain,
    expert_ids,
    route_weight,
    expert_gate,
    expert_up,
    expert_down,
    shared_gate,
    shared_up,
    shared_down,
):
    own_rows = tokens.shape[0]
    devices = lax.axis_size("ep")
    top_count = expert_ids.shape[1]
    capacity = max(2, 2 * own_rows * top_count // devices)
    inputs = tokens.astype(jnp.float32)
    normed = rms_scale(inputs, first_gain).astype(jnp.bfloat16)
    block_rows = lax.all_gather(normed, "ep", axis=0, tiled=True)
    columns = jnp.stack(
        [
            jnp.dot(block_rows, matrix, preferred_element_type=jnp.float32).astype(jnp.bfloat16)
            for matrix in (query_weight, key_weight, value_weight, outgate_weight)
        ]
    )
    projected = lax.all_to_all(columns, "ep", split_axis=1, concat_axis=2, tiled=True)
    gated, memory_next, norm_next, max_next = cell_step(
        normed,
        projected[0],
        projected[1],
        projected[2],
        projected[3],
        igate_weight,
        fgate_weight,
        igate_bias,
        fgate_bias,
        memory_state,
        norm_state,
        max_state,
        head_gain,
    )
    picked = gated
    mix_sums = jnp.dot(
        picked,
        lax.all_gather(out_weight, "ep", axis=0, tiled=True),
        preferred_element_type=jnp.float32,
    )
    stream = inputs + mix_sums.astype(jnp.bfloat16).astype(jnp.float32)
    normed_two = rms_scale(stream, second_gain).astype(jnp.bfloat16)
    block_rows = (
        lax.all_gather(shared_gate, "ep", axis=0, tiled=True),
        lax.all_gather(shared_up, "ep", axis=0, tiled=True),
    )
    picked = normed_two
    gate_shared = jnp.dot(picked, block_rows[0], preferred_element_type=jnp.float32)
    up_shared = jnp.dot(picked, block_rows[1], preferred_element_type=jnp.float32)
    hidden_shared = (jax.nn.silu(gate_shared) * up_shared).astype(jnp.bfloat16)
    shared_result = jnp.dot(
        hidden_shared,
        lax.all_gather(shared_down, "ep", axis=1, tiled=True),
        preferred_element_type=jnp.float32,
    )
    choose = (expert_ids[:, :, None] == jnp.arange(devices, dtype=jnp.int32)[None, None, :]).astype(
        jnp.int32
    )
    counted = jnp.sum(choose, axis=1)
    ranking = jnp.cumsum(counted, axis=0) - counted
    slot_index = jnp.sum(choose * ranking[:, None, :], axis=2)
    slot_ids = jnp.arange(capacity, dtype=jnp.int32)
    selector = counted.T[:, None, :] * (ranking.T[:, None, :] == slot_ids[None, :, None]).astype(
        jnp.int32
    )
    outgoing = jnp.einsum(
        "ecr,rd->ecd", selector.astype(jnp.bfloat16), normed_two, preferred_element_type=jnp.float32
    ).astype(jnp.bfloat16)
    arrived = lax.all_to_all(outgoing, "ep", split_axis=0, concat_axis=0, tiled=True)
    sources, slots, width = arrived.shape
    flat_rows = arrived.reshape(sources * slots, width)
    gate_sums = jnp.dot(flat_rows, expert_gate[0], preferred_element_type=jnp.float32)
    up_sums = jnp.dot(flat_rows, expert_up[0], preferred_element_type=jnp.float32)
    hidden = (jax.nn.silu(gate_sums) * up_sums).astype(jnp.bfloat16)
    result = jnp.dot(hidden, expert_down[0], preferred_element_type=jnp.float32).astype(
        jnp.bfloat16
    )
    results = lax.all_to_all(
        result.reshape(sources, slots, width), "ep", split_axis=0, concat_axis=0, tiled=True
    )
    flat_results = results.reshape(devices * capacity, results.shape[2])
    picked_results = flat_results[expert_ids * capacity + slot_index]
    routed = jnp.sum(route_weight[:, :, None] * picked_results.astype(jnp.float32), axis=1)
    mixed_out = (stream + routed + shared_result).astype(jnp.bfloat16)
    return (mixed_out, memory_next, norm_next, max_next)


ANY, VMEM = pl.ANY, pltpu.VMEM
F32, BF16 = jnp.float32, jnp.bfloat16


def across(left, right):
    return lax.dot_general(left, right, (((1,), (1,)), ((), ())), preferred_element_type=F32)


def turned_dot(left, right):
    return lax.dot_general(
        left.astype(BF16),
        right.astype(BF16),
        (((0,), (0,)), ((), ())),
        preferred_element_type=F32,
    )


def in_line(gain):
    held = gain[...].astype(F32)
    return jnp.concatenate([held[i : i + 1] for i in range(held.shape[0])], axis=1)


def offsets(chips):
    ring = chips // 2
    steps = [(step, flip) for step in range(ring) for flip in (1, 0) if step or flip]
    return sorted(steps, key=lambda o: -(min(o[0], ring - o[0]) + o[1]))


def fused(n, *refs):
    (tokens, first_gain, query_weight, key_weight, value_weight, outgate_weight, igate_weight,
     fgate_weight, igate_bias, fgate_bias, memory_state, norm_state, max_state, head_gain,
     out_weight, second_gain, expert_ids, route_weight, expert_gate, expert_up, expert_down,
     shared_gate, shared_up, shared_down,
     mixed_out, memory_next, norm_next, max_next,
     gain_one, gain_two, bias, gates_in, norm_in, max_in, gain_head, ids, route, sgate, sup, sdown,
     out_own, proj, wide, down, tok_all, table, normed, column_send, column_recv, gated_all,
     ow_all, mix_all, streamed, shared_send, shared_recv, sdown_recv, part, part_send, sum_recv,
     local_sem, memory_sem, send_sem, recv_sem, pair_send, pair_recv) = refs
    rows, width = tokens.shape
    heads, size = memory_state.shape[1], memory_state.shape[3]
    cut = query_weight.shape[0]
    chips = n // 2
    hidden = sgate.shape[1] // chips
    block = width // chips
    group = chips * rows
    top_count = expert_ids.shape[1]
    ring = chips // 2
    me = lax.axis_index("ep")
    side, chip = me % 2, me // 2
    partner = me + 1 - 2 * side
    order = offsets(chips)

    def to_chip(k):
        step, flip = order[k]
        return 2 * ((chip // 2 + step) % ring) + (chip + flip) % 2

    def from_chip(k):
        step, flip = order[k]
        return 2 * ((chip // 2 + ring - step) % ring) + (chip + flip) % 2

    barrier = pltpu.get_barrier_semaphore()
    for k in range(len(order)):
        pl.semaphore_signal(
            barrier,
            inc=1,
            device_id={"ep": 2 * to_chip(k) + side},
            device_id_type=pl.DeviceIdType.MESH,
        )
    pl.semaphore_signal(
        barrier, inc=1, device_id={"ep": partner}, device_id_type=pl.DeviceIdType.MESH
    )

    loads = []

    def load(source, target):
        copy = pltpu.make_async_copy(source, target, local_sem.at[len(loads)])
        copy.start()
        loads.append(copy)
        return copy

    token_load = load(tokens, tok_all.at[chip])
    gain_load = load(first_gain, gain_one)
    early = [
        load(igate_weight, gates_in.at[0]),
        load(fgate_weight, gates_in.at[1]),
        load(igate_bias, bias.at[0]),
        load(fgate_bias, bias.at[1]),
        load(max_state, max_in),
        load(expert_ids, ids),
        load(route_weight, route),
        load(shared_gate, sgate),
        load(shared_up, sup),
        load(shared_down, sdown),
        load(norm_state, norm_in),
        load(head_gain, gain_head),
        load(second_gain, gain_two),
    ]
    weights = (query_weight, key_weight, value_weight, outgate_weight)
    proj_loads = [load(matrix, proj.at[i, side]) for i, matrix in enumerate(weights)]
    out_load = load(out_weight, out_own)
    memory_loads = []
    for h in range(heads):
        copy = pltpu.make_async_copy(
            memory_state.at[:, h], memory_next.at[:, h], memory_sem.at[h]
        )
        copy.start()
        memory_loads.append(copy)
    columns_own = pl.ds(pl.multiple_of(chip * block, block), block)
    late = [
        load(out_weight.at[:, columns_own], ow_all.at[me]),
        load(expert_gate.at[0], wide.at[side, 0]),
        load(expert_up.at[0], wide.at[side, 1]),
        load(expert_down.at[0], down.at[side]),
    ]
    token_load.wait()
    unsent = []

    def spread(which, source, target):
        copies = []
        for k in range(len(order)):
            there = to_chip(k)
            copy = pltpu.make_async_remote_copy(
                src_ref=source(there),
                dst_ref=target,
                send_sem=send_sem.at[which, k],
                recv_sem=recv_sem.at[which, k],
                device_id={"ep": 2 * there + side},
                device_id_type=pl.DeviceIdType.MESH,
            )
            copy.start()
            copies.append(copy)
        unsent.extend(copies)
        return copies

    pairs = []

    def push(source, target):
        copy = pltpu.make_async_remote_copy(
            src_ref=source,
            dst_ref=target,
            send_sem=pair_send.at[len(pairs)],
            recv_sem=pair_recv.at[len(pairs)],
            device_id={"ep": partner},
            device_id_type=pl.DeviceIdType.MESH,
        )
        copy.start()
        pairs.append(copy)
        return copy

    pl.semaphore_wait(barrier, len(order) + 1)
    first = spread(0, lambda there: tok_all.at[chip], tok_all.at[chip])
    proj_pushes = [push(matrix, proj.at[i, side]) for i, matrix in enumerate(weights)]

    gain_load.wait()
    gain = in_line(gain_one)

    def norm_rows(source):
        values = rms_scale(tok_all[source].astype(F32), gain)
        normed[pl.ds(pl.multiple_of(source * rows, rows), rows), :] = values
        return values.astype(BF16)

    own = norm_rows(chip)
    for copy in early:
        copy.wait()
    lanes = lax.broadcasted_iota(jnp.int32, (rows, 128), 1)
    routes = jnp.zeros((rows, 128), F32)
    for t in range(top_count):
        routes = routes + jnp.where(ids[:, t : t + 1] == lanes, route[:, t : t + 1], 0.0)
    table[chip] = routes
    for i, matrix in enumerate((sgate, sup)):
        turned = matrix[...].astype(F32).T.reshape(chips, hidden, matrix.shape[0])
        shared_send[:, i * hidden : (i + 1) * hidden, :] = turned.astype(BF16)
    input_gate = across(own, gates_in[0]) + bias[0]
    forget_log = jax.nn.log_sigmoid(across(own, gates_in[1]) + bias[1])
    kept = forget_log + max_in[...]
    top = jnp.maximum(kept, input_gate)
    max_next[...] = top
    decay_rate = jnp.exp(kept - top)
    injected = jnp.exp(input_gate - top)
    floor = jnp.exp(-top)
    for copy in proj_loads:
        copy.wait()
    for copy in proj_pushes:
        copy.wait_recv()

    for k in reversed(range(len(order))):
        first[k].wait_recv()
        norm_rows(from_chip(k))

    columns = across(normed[...].astype(BF16), proj[...].reshape(8 * cut, width))
    column_send[...] = columns.reshape(chips, rows, 8 * cut).astype(BF16)
    second = spread(1, lambda there: column_send.at[there], column_recv.at[chip])
    column_recv[chip] = column_send[chip]
    out_load.wait()

    def out_columns(there):
        return out_own.at[:, pl.ds(pl.multiple_of(there * block, block), block)]

    out_spread = spread(2, out_columns, ow_all.at[me])
    table_spread = spread(3, lambda there: table.at[chip], table.at[chip])
    out_pushes = [push(out_columns(chip), ow_all.at[me])]
    expert_pushes = [
        push(expert_gate.at[0], wide.at[side, 0]),
        push(expert_up.at[0], wide.at[side, 1]),
        push(expert_down.at[0], down.at[side]),
    ]
    for k in range(len(order)):
        second[k].wait_recv()

    place = lax.broadcasted_iota(jnp.int32, (rows, rows * size), 1) // size
    diagonal = place == lax.broadcasted_iota(jnp.int32, (rows, rows * size), 0)
    ones = jnp.where(diagonal, 1.0, 0.0)
    blocks = jnp.concatenate([ones, jnp.zeros_like(ones)], axis=0)
    for h in range(heads):
        piece = column_recv[h].astype(F32)
        query, keyed, valued, outgate = [piece[:, i * size : (i + 1) * size] for i in range(4)]
        scale = injected[:, h : h + 1] * size ** (-0.5)
        decay = jnp.broadcast_to(decay_rate[:, h : h + 1], (rows, size))
        norm = decay * norm_in[:, h, :] + scale * keyed
        norm_next[:, h, :] = norm
        bottom = jnp.maximum(
            jnp.abs(jnp.sum(query * norm, axis=-1, keepdims=True)), floor[:, h : h + 1]
        )
        spread_value = jnp.where(diagonal, jnp.concatenate([scale * valued] * rows, axis=1), 0.0)
        high = spread_value.astype(BF16).astype(F32)
        outer = turned_dot(
            jnp.concatenate([keyed, keyed], axis=0),
            jnp.concatenate([high, spread_value - high], axis=0),
        )
        wide_query = turned_dot(jnp.concatenate([query, query * 0.0], axis=0), blocks)
        memory_loads[h].wait()
        tops = []
        for s in range(rows):
            cell = (
                decay[s : s + 1, :] * memory_next[s, h] + outer[:, s * size : (s + 1) * size]
            )
            memory_next[s, h] = cell
            tops.append(
                jnp.sum(wide_query[:, s * size : (s + 1) * size] * cell, axis=0, keepdims=True)
            )
        readout = jnp.concatenate(tops, axis=0) / bottom
        readout = rms_scale(readout, gain_head[h : h + 1, :])
        gated_all[chip, :, h * size : (h + 1) * size] = (
            readout * jax.nn.sigmoid(outgate)
        ).astype(BF16)

    third = spread(4, lambda there: gated_all.at[chip], gated_all.at[chip])
    for copy in late:
        copy.wait()
    for k in range(len(order)):
        out_spread[k].wait_recv()
        source = 2 * from_chip(k) + side
        out_pushes.append(push(ow_all.at[source], ow_all.at[source]))
    shared_spread = spread(5, lambda there: shared_send.at[there], shared_recv.at[me])
    shared_recv[me] = shared_send[chip]
    down_spread = spread(6, lambda there: sdown.at[there], sdown_recv.at[me])
    sdown_recv[me] = sdown[chip]
    shared_pushes = [
        push(shared_send.at[chip], shared_recv.at[me]),
        push(sdown.at[chip], sdown_recv.at[me]),
    ]
    for copy in out_pushes:
        copy.wait_recv()
    for k in range(len(order)):
        third[k].wait_recv()

    def flat(buffer):
        held = buffer[...].astype(F32)
        return held.reshape(group, held.shape[2])

    mix = jnp.dot(
        flat(gated_all).astype(BF16),
        ow_all[...].reshape(n * cut, block),
        preferred_element_type=F32,
    )
    mix_all[chip] = mix.astype(BF16)
    fourth = spread(7, lambda there: mix_all.at[chip], mix_all.at[chip])
    for k in range(len(order)):
        shared_spread[k].wait_recv()
        down_spread[k].wait_recv()
        source = 2 * from_chip(k) + side
        shared_pushes.append(push(shared_recv.at[source], shared_recv.at[source]))
        shared_pushes.append(push(sdown_recv.at[source], sdown_recv.at[source]))
    for k in range(len(order)):
        table_spread[k].wait_recv()
    weights_all = flat(table)
    expert_lane = lax.broadcasted_iota(jnp.int32, weights_all.shape, 1)
    for copy in shared_pushes + expert_pushes:
        copy.wait_recv()
    shared_wide = jnp.concatenate([shared_recv[i] for i in range(n)], axis=1)
    shared_rows = jnp.concatenate([sdown_recv[i] for i in range(n)], axis=1)
    for k in range(len(order)):
        fourth[k].wait_recv()

    stream = flat(tok_all) + jnp.concatenate(
        [mix_all[c].astype(F32) for c in range(chips)], axis=1
    )
    streamed[...] = stream.reshape(chips, rows, width)
    rows_two = rms_scale(stream, in_line(gain_two)).astype(BF16)
    both = across(rows_two, shared_wide)
    shared_hidden = (jax.nn.silu(both[:, :hidden]) * both[:, hidden:]).astype(BF16)
    value = jnp.dot(shared_hidden, shared_rows, preferred_element_type=F32)
    for e in range(2):
        gate_sums = jnp.dot(rows_two, wide[e, 0], preferred_element_type=F32)
        up_sums = jnp.dot(rows_two, wide[e, 1], preferred_element_type=F32)
        weight = jnp.sum(
            jnp.where(expert_lane == 2 * chip + e, weights_all, 0.0), axis=1, keepdims=True
        )
        own_hidden = (jax.nn.silu(gate_sums) * up_sums * weight).astype(BF16)
        value = value + jnp.dot(own_hidden, down[e], preferred_element_type=F32)
    part[...] = value.reshape(chips, rows, width)
    part_send[...] = value.reshape(chips, rows, width).astype(BF16)
    fifth = spread(8, lambda there: part_send.at[there], sum_recv.at[chip])
    total = streamed[chip] + part[chip]
    for k in reversed(range(len(order))):
        fifth[k].wait_recv()
        total = total + sum_recv[from_chip(k)].astype(F32)
    mixed_out[...] = total.astype(BF16)

    for copy in unsent + pairs:
        copy.wait_send()


def flush(*refs):
    sources, targets, sems = refs[:4], refs[4:8], refs[8]
    copies = []
    for i in (1, 2, 0, 3):
        if i == 1:
            for s in range(sources[i].shape[0]):
                copies.append((sources[i].at[s], targets[i].at[s]))
        else:
            copies.append((sources[i], targets[i]))
    started = []
    for i, (source, target) in enumerate(copies):
        copy = pltpu.make_async_copy(source, target, sems.at[i])
        copy.start()
        started.append(copy)
    for copy in started:
        copy.wait()


def fused_shards(n, *args):
    (tokens, first_gain, query_weight, key_weight, value_weight, outgate_weight, igate_weight,
     fgate_weight, igate_bias, fgate_bias, memory_state, norm_state, max_state, head_gain,
     out_weight, second_gain, expert_ids, route_weight, expert_gate, expert_up, expert_down,
     shared_gate, shared_up, shared_down) = args
    rows, width = tokens.shape
    heads, size = memory_state.shape[1], memory_state.shape[3]
    cut = query_weight.shape[1]
    chips = n // 2
    hidden = shared_gate.shape[1] // chips
    inner = expert_gate.shape[2]
    top_count = expert_ids.shape[1]
    deep = shared_gate.shape[0]
    lean = shared_down.shape[1]
    operands = (
        tokens, first_gain.reshape(-1, 128), query_weight.T, key_weight.T, value_weight.T,
        outgate_weight.T, igate_weight.T, fgate_weight.T, igate_bias.reshape(1, -1), fgate_bias.reshape(1, -1),
        memory_state, norm_state, max_state, head_gain.reshape(heads, size), out_weight,
        second_gain.reshape(-1, 128), expert_ids, route_weight, expert_gate, expert_up, expert_down,
        shared_gate, shared_up, shared_down.reshape(chips, hidden, lean),
    )
    operands = [pltpu.with_memory_space_constraint(x, pltpu.HBM) for x in operands]
    dma = pltpu.SemaphoreType.DMA
    results = (
        jax.ShapeDtypeStruct((rows, width), BF16),
        jax.ShapeDtypeStruct(memory_state.shape, F32),
        jax.ShapeDtypeStruct(norm_state.shape, F32),
        jax.ShapeDtypeStruct(max_state.shape, F32),
    )
    inside = pl.pallas_call(
        functools.partial(fused, n),
        out_shape=results,
        in_specs=[pl.BlockSpec(memory_space=pltpu.HBM)] * len(operands),
        out_specs=tuple(pl.BlockSpec(memory_space=VMEM) for _ in results),
        scratch_shapes=[
            VMEM((width // 128, 128), BF16),
            VMEM((width // 128, 128), BF16),
            VMEM((2, 1, heads), F32),
            VMEM((2, heads, width), BF16),
            VMEM(norm_state.shape, F32),
            VMEM(max_state.shape, F32),
            VMEM((heads, size), BF16),
            VMEM((rows, top_count), jnp.int32),
            VMEM((rows, top_count), F32),
            VMEM(shared_gate.shape, BF16),
            VMEM(shared_up.shape, BF16),
            VMEM((chips, hidden, lean), BF16),
            VMEM(out_weight.shape, BF16),
            VMEM((4, 2, cut, width), BF16),
            VMEM((2, 2, width, inner), BF16),
            VMEM((2, inner, width), BF16),
            VMEM((chips, rows, width), BF16),
            VMEM((chips, rows, 128), F32),
            VMEM((chips * rows, width), F32),
            VMEM((chips, rows, 8 * cut), BF16),
            VMEM((chips, rows, 8 * cut), BF16),
            VMEM((chips, rows, heads * size), BF16),
            VMEM((n, cut, width // chips), BF16),
            VMEM((chips, chips * rows, width // chips), BF16),
            VMEM((chips, rows, width), F32),
            VMEM((chips, 2 * hidden, deep), BF16),
            VMEM((n, 2 * hidden, deep), BF16),
            VMEM((n, hidden, lean), BF16),
            VMEM((chips, rows, width), F32),
            VMEM((chips, rows, width), BF16),
            VMEM((chips, rows, width), BF16),
            dma((32,)),
            dma((heads,)),
            dma((9, chips)),
            dma((9, chips)),
            dma((10 + 3 * chips,)),
            dma((10 + 3 * chips,)),
        ],
        compiler_params=pltpu.CompilerParams(
            collective_id=0, has_side_effects=True, vmem_limit_bytes=36 * 1024 * 1024
        ),
    )(*operands)
    return pl.pallas_call(
        flush,
        out_shape=results,
        in_specs=[pl.BlockSpec(memory_space=VMEM)] * 4,
        out_specs=tuple(pl.BlockSpec(memory_space=pltpu.HBM) for _ in results),
        scratch_shapes=[dma((rows + 3,))],
        compiler_params=pltpu.CompilerParams(vmem_limit_bytes=1024 * 1024),
    )(*[pltpu.with_memory_space_constraint(x, VMEM) for x in inside])


def fits(n, width, size, heads, cut, hidden_all, experts, rows):
    chips = n // 2
    return (
        n % 4 == 0
        and experts == n
        and heads == chips
        and 2 * cut == size
        and size == 128
        and width % (128 * n) == 0
        and hidden_all % (16 * chips) == 0
        and rows == 8
    )


def pick(n, *args):
    tokens, query_weight, memory_state = args[0], args[2], args[10]
    experts, hidden_all = args[18].shape[0] * n, args[21].shape[1]
    if fits(
        n, tokens.shape[1], memory_state.shape[3], memory_state.shape[1], query_weight.shape[1],
        hidden_all, experts, tokens.shape[0],
    ):
        return fused_shards(n, *args)
    return shards(*args)


def solution(mesh):
    placed = (
        P(("grp", "ep"), None),
        P(),
        P(None, "ep"),
        P(None, "ep"),
        P(None, "ep"),
        P(None, "ep"),
        P(),
        P(),
        P(),
        P(),
        P(("grp", "ep"), None, None, None),
        P(("grp", "ep"), None, None),
        P(("grp", "ep"), None),
        P(),
        P("ep", None),
        P(),
        P(("grp", "ep"), None),
        P(("grp", "ep"), None),
        P("ep", None, None),
        P("ep", None, None),
        P("ep", None, None),
        P("ep", None),
        P("ep", None),
        P(None, "ep"),
    )
    return jax.shard_map(
        functools.partial(pick, mesh.shape["ep"]),
        mesh=mesh,
        in_specs=placed,
        out_specs=(
            P(("grp", "ep"), None),
            P(("grp", "ep"), None, None, None),
            P(("grp", "ep"), None, None),
            P(("grp", "ep"), None),
        ),
        check_vma=False,
    )
```

time: 60.8 us -> 48.7 us (0.80)
  Pallas kernels: 56.1 us -> 47.9 us
  local copies, waits for them, and re-layouts: 3.84 us -> 0 us
    pallas_call x1 -> x2, Pallas kernels: 56.1 us -> 47.9 us  [the longest x1 45.8 us: fused_shards(): pl.pallas_call(functools.partial(fused, n), out_shape=results, in_specs=[...]
    unnamed x4 -> x0, local copies, waits for them, and re-layouts: 3.84 us -> none
where the time goes in v2:
time: 48.7 us; the launch traced here: 48.5 us
  Pallas kernels  47.9 us (98%)
  between operations  0.65 us (1%)
    pallas_call x1, Pallas kernels, fused_shards(): pl.pallas_call(functools.partial(fused, n), out_shape=results, in_specs=[...  45.8 us
    pallas_call x1, Pallas kernels, fused_shards(): pl.pallas_call(flush, out_shape=results, in_specs=[pl.BlockSpec(memory_sp...  2.11 us

profile of v2, /device:TPU:0, one launch (start us, length us, event | category | flops | bytes accessed | tf_op | source)
XLA Modules:
  0.0 48.5 jit_solution(3445507799863562993)
XLA Ops:
  0.6 45.8 %shard_map.255 = (bf16[8,2048]{1,0:T(8,128)(2,1)S(1)}, f32[8,8,128,128]{3,2,1,0:T(8,128)S(1)}, f32[8,8,128]{2,1,0:T(8,128)S(1)}, f32[8,8]{1,0:T(8,128)S(1)}) custom-call(bf16[8,2048]{1,0:T(8,128)(2,1)} %refs_0_.1, bf16[16,128]{1,0:T(8,128)(2,1)} %bitcast.19, bf16[64,2048]{1,0:T(8,128)(2,1)} %bitcast.12, bf16[64,2048]{1,0:T(8,128)(2,1)} %bitcast.13, ...), custom_call_target="tpu_custom_call" | custom-call | tf_op jit(solution)/shard_map/pallas_call | solution.py:545
  46.4 2.1 %shard_map.256 = (bf16[8,2048]{1,0:T(8,128)(2,1)}, f32[8,8,128,128]{3,2,1,0:T(8,128)}, f32[8,8,128]{2,1,0:T(8,128)}, f32[8,8]{1,0:T(8,128)}) custom-call(bf16[8,2048]{1,0:T(8,128)(2,1)S(1)} %get-tuple-element.8.refs_0_, f32[8,8,128,128]{3,2,1,0:T(8,128)S(1)} %get-tuple-element.9.refs_1_, f32[8,8,128]{2,1,0:T(8,128)S(1)} %get-tuple-element.10.refs_2_, ...), custom_call_target="tpu_custom_call" | custom-call | tf_op jit(solution)/shard_map/pallas_call | solution.py:593

commit v3 on v2

--- a/solution.py
+++ b/solution.py
@@ -206,10 +206,10 @@
      out_weight, second_gain, expert_ids, route_weight, expert_gate, expert_up, expert_down,
      shared_gate, shared_up, shared_down,
      mixed_out, memory_next, norm_next, max_next,
-     gain_one, gain_two, bias, gates_in, norm_in, max_in, gain_head, ids, route, sgate, sup, sdown,
+     gain_one, gain_two, bias, gates_in, norm_in, max_in, gain_head, ids, route, sgate, sup,
      out_own, proj, wide, down, tok_all, table, normed, column_send, column_recv, gated_all,
-     ow_all, mix_all, streamed, shared_send, shared_recv, sdown_recv, part, part_send, sum_recv,
-     local_sem, memory_sem, send_sem, recv_sem, pair_send, pair_recv) = refs
+     ow_all, mix_all, streamed, pack_send, pack_recv, part, part_send, sum_recv, gain_rows, sums_all,
+     local_sem, memory_sem, send_sem, recv_sem, pair_send, pair_recv, twin_send, twin_recv) = refs
     rows, width = tokens.shape
     heads, size = memory_state.shape[1], memory_state.shape[3]
     cut = query_weight.shape[0]
@@ -220,6 +220,8 @@
     top_count = expert_ids.shape[1]
     ring = chips // 2
     me = lax.axis_index("ep")
+    plane = lax.axis_index("grp")
+    other = 1 - plane
     side, chip = me % 2, me // 2
     partner = me + 1 - 2 * side
     order = offsets(chips)
@@ -244,6 +246,9 @@
         barrier, inc=1, device_id={"ep": partner}, device_id_type=pl.DeviceIdType.MESH
     )
 
+    pl.semaphore_signal(
+        barrier, inc=1, device_id={"grp": other}, device_id_type=pl.DeviceIdType.MESH
+    )
     loads = []
 
     def load(source, target):
@@ -264,14 +269,22 @@
         load(route_weight, route),
         load(shared_gate, sgate),
         load(shared_up, sup),
-        load(shared_down, sdown),
+        load(shared_down.at[:, 0], pack_send.at[:, 0, hidden:]),
+        load(shared_down.at[:, 1], pack_send.at[:, 1, hidden:]),
         load(norm_state, norm_in),
         load(head_gain, gain_head),
         load(second_gain, gain_two),
     ]
     weights = (query_weight, key_weight, value_weight, outgate_weight)
     proj_loads = [load(matrix, proj.at[i, side]) for i, matrix in enumerate(weights)]
-    out_load = load(out_weight, out_own)
+    out_loads = [
+        load(
+            out_weight.at[i * cut // 2 : (i + 1) * cut // 2, pl.ds(c * block, block)],
+            out_own.at[c, i],
+        )
+        for c in range(chips)
+        for i in range(2)
+    ]
     memory_loads = []
     for h in range(heads):
         copy = pltpu.make_async_copy(
@@ -279,9 +292,7 @@
         )
         copy.start()
         memory_loads.append(copy)
-    columns_own = pl.ds(pl.multiple_of(chip * block, block), block)
     late = [
-        load(out_weight.at[:, columns_own], ow_all.at[me]),
         load(expert_gate.at[0], wide.at[side, 0]),
         load(expert_up.at[0], wide.at[side, 1]),
         load(expert_down.at[0], down.at[side]),
@@ -306,6 +317,21 @@
         unsent.extend(copies)
         return copies
 
+    twins = []
+
+    def cross(source, target):
+        copy = pltpu.make_async_remote_copy(
+            src_ref=source,
+            dst_ref=target,
+            send_sem=twin_send.at[len(twins)],
+            recv_sem=twin_recv.at[len(twins)],
+            device_id={"grp": other},
+            device_id_type=pl.DeviceIdType.MESH,
+        )
+        copy.start()
+        twins.append(copy)
+        return copy
+
     pairs = []
 
     def push(source, target):
@@ -321,10 +347,24 @@
         pairs.append(copy)
         return copy
 
-    pl.semaphore_wait(barrier, len(order) + 1)
+    drained = [0, 0, 0]
+
+    def drain(keep=0):
+        for i, held in enumerate((unsent, pairs, twins)):
+            stop = len(held) - (keep if i == 0 else 0)
+            for copy in held[drained[i] : stop]:
+                copy.wait_send()
+            drained[i] = stop
+
+    pl.semaphore_wait(barrier, len(order) + 2)
     first = spread(0, lambda there: tok_all.at[chip], tok_all.at[chip])
     proj_pushes = [push(matrix, proj.at[i, side]) for i, matrix in enumerate(weights)]
 
+    expert_pushes = [
+        push(expert_gate.at[0], wide.at[side, 0]),
+        push(expert_up.at[0], wide.at[side, 1]),
+        push(expert_down.at[0], down.at[side]),
+    ]
     gain_load.wait()
     gain = in_line(gain_one)
 
@@ -336,14 +376,17 @@
     own = norm_rows(chip)
     for copy in early:
         copy.wait()
-    lanes = lax.broadcasted_iota(jnp.int32, (rows, 128), 1)
-    routes = jnp.zeros((rows, 128), F32)
+    lanes = lax.broadcasted_iota(jnp.int32, (rows, rows * n), 1)
+    mine = lanes // n == lax.broadcasted_iota(jnp.int32, (rows, rows * n), 0)
+    routes = jnp.zeros((rows, rows * n), F32)
     for t in range(top_count):
-        routes = routes + jnp.where(ids[:, t : t + 1] == lanes, route[:, t : t + 1], 0.0)
-    table[chip] = routes
+        routes = routes + jnp.where(
+            mine & (lanes % n == ids[:, t : t + 1]), route[:, t : t + 1], 0.0
+        )
+    table[chip] = jnp.sum(routes, axis=0, keepdims=True)
     for i, matrix in enumerate((sgate, sup)):
         turned = matrix[...].astype(F32).T.reshape(chips, hidden, matrix.shape[0])
-        shared_send[:, i * hidden : (i + 1) * hidden, :] = turned.astype(BF16)
+        pack_send[:, i, :hidden, :] = turned.astype(BF16)
     input_gate = across(own, gates_in[0]) + bias[0]
     forget_log = jax.nn.log_sigmoid(across(own, gates_in[1]) + bias[1])
     kept = forget_log + max_in[...]
@@ -365,26 +408,35 @@
     column_send[...] = columns.reshape(chips, rows, 8 * cut).astype(BF16)
     second = spread(1, lambda there: column_send.at[there], column_recv.at[chip])
     column_recv[chip] = column_send[chip]
-    out_load.wait()
-
-    def out_columns(there):
-        return out_own.at[:, pl.ds(pl.multiple_of(there * block, block), block)]
-
-    out_spread = spread(2, out_columns, ow_all.at[me])
+    for copy in out_loads:
+        copy.wait()
+    out_spread = spread(2, lambda there: out_own.at[there, plane], ow_all.at[me, plane])
     table_spread = spread(3, lambda there: table.at[chip], table.at[chip])
-    out_pushes = [push(out_columns(chip), ow_all.at[me])]
-    expert_pushes = [
-        push(expert_gate.at[0], wide.at[side, 0]),
-        push(expert_up.at[0], wide.at[side, 1]),
-        push(expert_down.at[0], down.at[side]),
-    ]
+    near_pushes = [push(out_own.at[chip], ow_all.at[me]), push(pack_send.at[chip], pack_recv.at[me])]
+    ow_all[me] = out_own[chip]
+    pack_recv[me] = pack_send[chip]
+    out_pushes, pack_pushes, out_twins, pack_twins = [], [], [], []
+
+    def forward(copies, buffer, crossed, pushed):
+        for k in range(len(order)):
+            copies[k].wait_recv()
+            held = buffer.at[2 * from_chip(k) + side, plane]
+            crossed.append(cross(held, held))
+            pushed.append(push(held, held))
+
+    def settle(crossed, buffer, pushed):
+        for k in range(len(order)):
+            crossed[k].wait_recv()
+            held = buffer.at[2 * from_chip(k) + side, other]
+            pushed.append(push(held, held))
+
+    for copy in memory_loads:
+        copy.wait()
     for k in range(len(order)):
         second[k].wait_recv()
 
     place = lax.broadcasted_iota(jnp.int32, (rows, rows * size), 1) // size
     diagonal = place == lax.broadcasted_iota(jnp.int32, (rows, rows * size), 0)
-    ones = jnp.where(diagonal, 1.0, 0.0)
-    blocks = jnp.concatenate([ones, jnp.zeros_like(ones)], axis=0)
     for h in range(heads):
         piece = column_recv[h].astype(F32)
         query, keyed, valued, outgate = [piece[:, i * size : (i + 1) * size] for i in range(4)]
@@ -401,39 +453,28 @@
             jnp.concatenate([keyed, keyed], axis=0),
             jnp.concatenate([high, spread_value - high], axis=0),
         )
-        wide_query = turned_dot(jnp.concatenate([query, query * 0.0], axis=0), blocks)
-        memory_loads[h].wait()
+        query_columns = query.T
         tops = []
         for s in range(rows):
             cell = (
                 decay[s : s + 1, :] * memory_next[s, h] + outer[:, s * size : (s + 1) * size]
             )
             memory_next[s, h] = cell
-            tops.append(
-                jnp.sum(wide_query[:, s * size : (s + 1) * size] * cell, axis=0, keepdims=True)
-            )
+            tops.append(jnp.sum(query_columns[:, s : s + 1] * cell, axis=0, keepdims=True))
         readout = jnp.concatenate(tops, axis=0) / bottom
         readout = rms_scale(readout, gain_head[h : h + 1, :])
         gated_all[chip, :, h * size : (h + 1) * size] = (
             readout * jax.nn.sigmoid(outgate)
         ).astype(BF16)
+        if h == heads // 2:
+            forward(out_spread, ow_all, out_twins, out_pushes)
 
     third = spread(4, lambda there: gated_all.at[chip], gated_all.at[chip])
     for copy in late:
         copy.wait()
-    for k in range(len(order)):
-        out_spread[k].wait_recv()
-        source = 2 * from_chip(k) + side
-        out_pushes.append(push(ow_all.at[source], ow_all.at[source]))
-    shared_spread = spread(5, lambda there: shared_send.at[there], shared_recv.at[me])
-    shared_recv[me] = shared_send[chip]
-    down_spread = spread(6, lambda there: sdown.at[there], sdown_recv.at[me])
-    sdown_recv[me] = sdown[chip]
-    shared_pushes = [
-        push(shared_send.at[chip], shared_recv.at[me]),
-        push(sdown.at[chip], sdown_recv.at[me]),
-    ]
-    for copy in out_pushes:
+    pack_spread = spread(5, lambda there: pack_send.at[there, plane], pack_recv.at[me, plane])
+    settle(out_twins, ow_all, out_pushes)
+    for copy in near_pushes + out_pushes:
         copy.wait_recv()
     for k in range(len(order)):
         third[k].wait_recv()
@@ -449,50 +490,103 @@
     )
     mix_all[chip] = mix.astype(BF16)
     fourth = spread(7, lambda there: mix_all.at[chip], mix_all.at[chip])
-    for k in range(len(order)):
-        shared_spread[k].wait_recv()
-        down_spread[k].wait_recv()
-        source = 2 * from_chip(k) + side
-        shared_pushes.append(push(shared_recv.at[source], shared_recv.at[source]))
-        shared_pushes.append(push(sdown_recv.at[source], sdown_recv.at[source]))
+    drain(2 * len(order))
+    forward(pack_spread, pack_recv, pack_twins, pack_pushes)
+    settle(pack_twins, pack_recv, pack_pushes)
     for k in range(len(order)):
         table_spread[k].wait_recv()
-    weights_all = flat(table)
-    expert_lane = lax.broadcasted_iota(jnp.int32, weights_all.shape, 1)
-    for copy in shared_pushes + expert_pushes:
+    for copy in pack_pushes + expert_pushes:
         copy.wait_recv()
-    shared_wide = jnp.concatenate([shared_recv[i] for i in range(n)], axis=1)
-    shared_rows = jnp.concatenate([sdown_recv[i] for i in range(n)], axis=1)
-    for k in range(len(order)):
+    gain = in_line(gain_two)
+    gain_rows[...] = gain.reshape(chips, 1, block)
+
+    def take(source):
+        span = pl.ds(pl.multiple_of(source * block, block), block)
+        held = tok_all[:, :, span].astype(F32).reshape(group, block) + mix_all[source].astype(F32)
+        streamed[:, :, span] = held.reshape(chips, rows, block)
+        scaled = (held * gain_rows[source]).astype(BF16)
+        parts = [
+            jnp.dot(scaled, wide[e, i, span, :], preferred_element_type=F32)
+            for e in range(2)
+            for i in range(2)
+        ]
+        turned = jnp.concatenate(
+            [
+                jnp.concatenate([pack_recv[2 * source + j, i, :hidden, :] for i in range(2)], axis=0)
+                for j in range(2)
+            ],
+            axis=1,
+        )
+        return parts + [across(scaled, turned)], jnp.sum(held * held, axis=1, keepdims=True)
+
+    inner = wide.shape[3]
+    spots = [i * inner for i in range(5)]
+
+    def keep(source, fresh):
+        parts, squares = take(source)
+        for spot, value in zip(spots, parts):
+            here = slice(spot, spot + value.shape[1])
+            sums_all[:, here] = value if fresh else sums_all[:, here] + value
+        return squares
+
+    squares = keep(chip, True)
+    lane_at = lax.broadcasted_iota(jnp.int32, (group, rows * n), 1)
+    row_at = lax.broadcasted_iota(jnp.int32, (group, rows * n), 0) % rows
+    weights_all = jnp.concatenate(
+        [jnp.broadcast_to(table[c], (rows, rows * n)) for c in range(chips)], axis=0
+    )
+    routed = [
+        jnp.sum(
+            jnp.where(lane_at == row_at * n + 2 * chip + e, weights_all, 0.0),
+            axis=1,
+            keepdims=True,
+        )
+        for e in range(2)
+    ]
+    shared_rows = jnp.concatenate(
+        [
+            jnp.concatenate([pack_recv[i, j, hidden:, :] for i in range(n)], axis=1)
+            for j in range(2)
+        ],
+        axis=0,
+    )
+    for k in reversed(range(len(order))):
         fourth[k].wait_recv()
-
-    stream = flat(tok_all) + jnp.concatenate(
-        [mix_all[c].astype(F32) for c in range(chips)], axis=1
-    )
-    streamed[...] = stream.reshape(chips, rows, width)
-    rows_two = rms_scale(stream, in_line(gain_two)).astype(BF16)
-    both = across(rows_two, shared_wide)
+        squares = squares + keep(from_chip(k), False)
+
+    scale = lax.rsqrt(squares / width + epsilon)
+    hiddens = []
+    for e in range(2):
+        gate_sums = sums_all[:, spots[2 * e] : spots[2 * e] + inner] * scale
+        up_sums = sums_all[:, spots[2 * e + 1] : spots[2 * e + 1] + inner] * scale
+        hiddens.append((jax.nn.silu(gate_sums) * up_sums * routed[e]).astype(BF16))
+    both = sums_all[:, spots[4] : spots[4] + 2 * hidden] * scale
     shared_hidden = (jax.nn.silu(both[:, :hidden]) * both[:, hidden:]).astype(BF16)
-    value = jnp.dot(shared_hidden, shared_rows, preferred_element_type=F32)
-    for e in range(2):
-        gate_sums = jnp.dot(rows_two, wide[e, 0], preferred_element_type=F32)
-        up_sums = jnp.dot(rows_two, wide[e, 1], preferred_element_type=F32)
-        weight = jnp.sum(
-            jnp.where(expert_lane == 2 * chip + e, weights_all, 0.0), axis=1, keepdims=True
-        )
-        own_hidden = (jax.nn.silu(gate_sums) * up_sums * weight).astype(BF16)
-        value = value + jnp.dot(own_hidden, down[e], preferred_element_type=F32)
-    part[...] = value.reshape(chips, rows, width)
-    part_send[...] = value.reshape(chips, rows, width).astype(BF16)
-    fifth = spread(8, lambda there: part_send.at[there], sum_recv.at[chip])
-    total = streamed[chip] + part[chip]
-    for k in reversed(range(len(order))):
-        fifth[k].wait_recv()
-        total = total + sum_recv[from_chip(k)].astype(F32)
-    mixed_out[...] = total.astype(BF16)
-
-    for copy in unsent + pairs:
-        copy.wait_send()
+    half = width // 2
+    fifth = []
+    for i in range(2):
+        span = slice(i * half, (i + 1) * half)
+        value = jnp.dot(shared_hidden, shared_rows[:, span], preferred_element_type=F32)
+        for e in range(2):
+            value = value + jnp.dot(hiddens[e], down[e, :, span], preferred_element_type=F32)
+        value = value.reshape(chips, rows, half)
+        part[i] = value
+        part_send[i] = value.astype(BF16)
+        fifth.append(
+            spread(
+                (8, 9)[i], lambda there: part_send.at[i, there], sum_recv.at[i, chip]
+            )
+        )
+    drain(2 * len(order))
+    for i in range(2):
+        span = slice(i * half, (i + 1) * half)
+        total = streamed[chip, :, span] + part[i, chip]
+        for k in reversed(range(len(order))):
+            fifth[i][k].wait_recv()
+            total = total + sum_recv[i, from_chip(k)].astype(F32)
+        mixed_out[:, span] = total.astype(BF16)
+
+    drain()
 
 
 def flush(*refs):
@@ -525,14 +619,13 @@
     hidden = shared_gate.shape[1] // chips
     inner = expert_gate.shape[2]
     top_count = expert_ids.shape[1]
-    deep = shared_gate.shape[0]
     lean = shared_down.shape[1]
     operands = (
         tokens, first_gain.reshape(-1, 128), query_weight.T, key_weight.T, value_weight.T,
         outgate_weight.T, igate_weight.T, fgate_weight.T, igate_bias.reshape(1, -1), fgate_bias.reshape(1, -1),
         memory_state, norm_state, max_state, head_gain.reshape(heads, size), out_weight,
         second_gain.reshape(-1, 128), expert_ids, route_weight, expert_gate, expert_up, expert_down,
-        shared_gate, shared_up, shared_down.reshape(chips, hidden, lean),
+        shared_gate, shared_up, shared_down.reshape(chips, 2, hidden // 2, lean),
     )
     operands = [pltpu.with_memory_space_constraint(x, pltpu.HBM) for x in operands]
     dma = pltpu.SemaphoreType.DMA
@@ -559,32 +652,34 @@
             VMEM((rows, top_count), F32),
             VMEM(shared_gate.shape, BF16),
             VMEM(shared_up.shape, BF16),
-            VMEM((chips, hidden, lean), BF16),
-            VMEM(out_weight.shape, BF16),
+            VMEM((chips, 2, cut // 2, width // chips), BF16),
             VMEM((4, 2, cut, width), BF16),
             VMEM((2, 2, width, inner), BF16),
             VMEM((2, inner, width), BF16),
             VMEM((chips, rows, width), BF16),
-            VMEM((chips, rows, 128), F32),
+            VMEM((chips, 1, rows * n), F32),
             VMEM((chips * rows, width), F32),
             VMEM((chips, rows, 8 * cut), BF16),
             VMEM((chips, rows, 8 * cut), BF16),
             VMEM((chips, rows, heads * size), BF16),
-            VMEM((n, cut, width // chips), BF16),
+            VMEM((n, 2, cut // 2, width // chips), BF16),
             VMEM((chips, chips * rows, width // chips), BF16),
             VMEM((chips, rows, width), F32),
-            VMEM((chips, 2 * hidden, deep), BF16),
-            VMEM((n, 2 * hidden, deep), BF16),
-            VMEM((n, hidden, lean), BF16),
-            VMEM((chips, rows, width), F32),
-            VMEM((chips, rows, width), BF16),
-            VMEM((chips, rows, width), BF16),
-            dma((32,)),
+            VMEM((chips, 2, 3 * hidden // 2, lean), BF16),
+            VMEM((n, 2, 3 * hidden // 2, lean), BF16),
+            VMEM((2, chips, rows, width // 2), F32),
+            VMEM((2, chips, rows, width // 2), BF16),
+            VMEM((2, chips, rows, width // 2), BF16),
+            VMEM((chips, 1, width // chips), F32),
+            VMEM((chips * rows, 4 * inner + 128), F32),
+            dma((24 + 2 * chips,)),
             dma((heads,)),
-            dma((9, chips)),
-            dma((9, chips)),
-            dma((10 + 3 * chips,)),
-            dma((10 + 3 * chips,)),
+            dma((10, chips)),
+            dma((10, chips)),
+            dma((10 + 4 * chips,)),
+            dma((10 + 4 * chips,)),
+            dma((2 * chips,)),
+            dma((2 * chips,)),
         ],
         compiler_params=pltpu.CompilerParams(
             collective_id=0, has_side_effects=True, vmem_limit_bytes=36 * 1024 * 1024
@@ -600,25 +695,28 @@
     )(*[pltpu.with_memory_space_constraint(x, VMEM) for x in inside])
 
 
-def fits(n, width, size, heads, cut, hidden_all, experts, rows):
+def fits(n, groups, width, size, heads, cut, hidden_all, experts, rows):
     chips = n // 2
     return (
         n % 4 == 0
+        and groups == 2
+        and rows * n == 128
         and experts == n
         and heads == chips
         and 2 * cut == size
         and size == 128
         and width % (128 * n) == 0
-        and hidden_all % (16 * chips) == 0
+        and hidden_all % (32 * chips) == 0
         and rows == 8
-    )
-
-
-def pick(n, *args):
+        and 2 * hidden_all <= 128 * chips
+    )
+
+
+def pick(n, groups, *args):
     tokens, query_weight, memory_state = args[0], args[2], args[10]
     experts, hidden_all = args[18].shape[0] * n, args[21].shape[1]
     if fits(
-        n, tokens.shape[1], memory_state.shape[3], memory_state.shape[1], query_weight.shape[1],
+        n, groups, tokens.shape[1], memory_state.shape[3], memory_state.shape[1], query_weight.shape[1],
         hidden_all, experts, tokens.shape[0],
     ):
         return fused_shards(n, *args)
@@ -653,7 +751,7 @@
         P(None, "ep"),
     )
     return jax.shard_map(
-        functools.partial(pick, mesh.shape["ep"]),
+        functools.partial(pick, mesh.shape["ep"], mesh.shape["grp"]),
         mesh=mesh,
         in_specs=placed,
         out_specs=(

time: 48.7 us -> 46.9 us (0.963)
  Pallas kernels: 47.9 us -> 46.1 us
    pallas_call x1, Pallas kernels: 45.8 us -> 44 us  [fused_shards(): pl.pallas_call(functools.partial(fused, n), out_shape=results, in_specs=[...]
where the time goes in v3:
time: 46.9 us; the launch traced here: 46.8 us
  Pallas kernels  46.1 us (98%)
  between operations  0.65 us (1%)
    pallas_call x1, Pallas kernels, fused_shards(): pl.pallas_call(functools.partial(fused, n), out_shape=results, in_specs=[...  44 us
    pallas_call x1, Pallas kernels, fused_shards(): pl.pallas_call(flush, out_shape=results, in_specs=[pl.BlockSpec(memory_sp...  2.11 us

profile of v3, /device:TPU:0, one launch (start us, length us, event | category | flops | bytes accessed | tf_op | source)
XLA Modules:
  0.0 46.8 jit_solution(12952852680062766837)
XLA Ops:
  0.6 44.0 %shard_map.255 = (bf16[8,2048]{1,0:T(8,128)(2,1)S(1)}, f32[8,8,128,128]{3,2,1,0:T(8,128)S(1)}, f32[8,8,128]{2,1,0:T(8,128)S(1)}, f32[8,8]{1,0:T(8,128)S(1)}) custom-call(bf16[8,2048]{1,0:T(8,128)(2,1)} %refs_0_.1, bf16[16,128]{1,0:T(8,128)(2,1)} %bitcast.19, bf16[64,2048]{1,0:T(8,128)(2,1)} %bitcast.12, bf16[64,2048]{1,0:T(8,128)(2,1)} %bitcast.13, ...), custom_call_target="tpu_custom_call" | custom-call | tf_op jit(solution)/shard_map/pallas_call | solution.py:638
  44.7 2.1 %shard_map.256 = (bf16[8,2048]{1,0:T(8,128)(2,1)}, f32[8,8,128,128]{3,2,1,0:T(8,128)}, f32[8,8,128]{2,1,0:T(8,128)}, f32[8,8]{1,0:T(8,128)}) custom-call(bf16[8,2048]{1,0:T(8,128)(2,1)S(1)} %get-tuple-element.8.refs_0_, f32[8,8,128,128]{3,2,1,0:T(8,128)S(1)} %get-tuple-element.9.refs_1_, f32[8,8,128]{2,1,0:T(8,128)S(1)} %get-tuple-element.10.refs_2_, ...), custom_call_target="tpu_custom_call" | custom-call | tf_op jit(solution)/shard_map/pallas_call | solution.py:688

commit v4 on v3

--- a/solution.py
+++ b/solution.py
@@ -277,21 +277,14 @@
     ]
     weights = (query_weight, key_weight, value_weight, outgate_weight)
     proj_loads = [load(matrix, proj.at[i, side]) for i, matrix in enumerate(weights)]
-    out_loads = [
-        load(
-            out_weight.at[i * cut // 2 : (i + 1) * cut // 2, pl.ds(c * block, block)],
-            out_own.at[c, i],
-        )
-        for c in range(chips)
-        for i in range(2)
-    ]
+    out_load = load(out_weight, out_own)
     memory_loads = []
-    for h in range(heads):
-        copy = pltpu.make_async_copy(
-            memory_state.at[:, h], memory_next.at[:, h], memory_sem.at[h]
-        )
-        copy.start()
-        memory_loads.append(copy)
+    for i in range(4):
+        some = pl.ds(i * rows // 4, rows // 4)
+        memory_loads.append(
+            pltpu.make_async_copy(memory_state.at[some], memory_next.at[some], memory_sem.at[i])
+        )
+        memory_loads[i].start()
     late = [
         load(expert_gate.at[0], wide.at[side, 0]),
         load(expert_up.at[0], wide.at[side, 1]),
@@ -352,9 +345,9 @@
     def drain(keep=0):
         for i, held in enumerate((unsent, pairs, twins)):
             stop = len(held) - (keep if i == 0 else 0)
-            for copy in held[drained[i] : stop]:
+            for copy in held[drained[i] : stop] if i == 0 or not keep else []:
                 copy.wait_send()
-            drained[i] = stop
+                drained[i] += 1
 
     pl.semaphore_wait(barrier, len(order) + 2)
     first = spread(0, lambda there: tok_all.at[chip], tok_all.at[chip])
@@ -408,27 +401,30 @@
     column_send[...] = columns.reshape(chips, rows, 8 * cut).astype(BF16)
     second = spread(1, lambda there: column_send.at[there], column_recv.at[chip])
     column_recv[chip] = column_send[chip]
-    for copy in out_loads:
-        copy.wait()
-    out_spread = spread(2, lambda there: out_own.at[there, plane], ow_all.at[me, plane])
+    out_load.wait()
+
+    def out_columns(there):
+        rows_here = pl.ds(pl.multiple_of(plane * (cut // 2), cut // 2), cut // 2)
+        return out_own.at[rows_here, pl.ds(pl.multiple_of(there * block, block), block)]
+
+    out_spread = spread(2, out_columns, ow_all.at[chip, side, plane])
     table_spread = spread(3, lambda there: table.at[chip], table.at[chip])
-    near_pushes = [push(out_own.at[chip], ow_all.at[me]), push(pack_send.at[chip], pack_recv.at[me])]
-    ow_all[me] = out_own[chip]
-    pack_recv[me] = pack_send[chip]
+    ow_all[chip, side, plane] = out_columns(chip)[...]
+    pack_recv[chip, side, plane] = pack_send[chip, plane]
     out_pushes, pack_pushes, out_twins, pack_twins = [], [], [], []
 
     def forward(copies, buffer, crossed, pushed):
-        for k in range(len(order)):
-            copies[k].wait_recv()
-            held = buffer.at[2 * from_chip(k) + side, plane]
-            crossed.append(cross(held, held))
-            pushed.append(push(held, held))
+        for copy in copies:
+            copy.wait_recv()
+        held = buffer.at[:, side, plane]
+        crossed.append(cross(held, held))
+        pushed.append(push(held, held))
 
     def settle(crossed, buffer, pushed):
-        for k in range(len(order)):
-            crossed[k].wait_recv()
-            held = buffer.at[2 * from_chip(k) + side, other]
-            pushed.append(push(held, held))
+        for copy in crossed:
+            copy.wait_recv()
+        held = buffer.at[:, side, other]
+        pushed.append(push(held, held))
 
     for copy in memory_loads:
         copy.wait()
@@ -469,12 +465,13 @@
         if h == heads // 2:
             forward(out_spread, ow_all, out_twins, out_pushes)
 
-    third = spread(4, lambda there: gated_all.at[chip], gated_all.at[chip])
+    drain(len(unsent) - len(order))
+    third = spread(0, lambda there: gated_all.at[chip], gated_all.at[chip])
     for copy in late:
         copy.wait()
-    pack_spread = spread(5, lambda there: pack_send.at[there, plane], pack_recv.at[me, plane])
+    pack_spread = spread(4, lambda there: pack_send.at[there, plane], pack_recv.at[chip, side, plane])
     settle(out_twins, ow_all, out_pushes)
-    for copy in near_pushes + out_pushes:
+    for copy in out_pushes:
         copy.wait_recv()
     for k in range(len(order)):
         third[k].wait_recv()
@@ -489,7 +486,8 @@
         preferred_element_type=F32,
     )
     mix_all[chip] = mix.astype(BF16)
-    fourth = spread(7, lambda there: mix_all.at[chip], mix_all.at[chip])
+    drain(len(unsent) - 2 * len(order))
+    fourth = spread(1, lambda there: mix_all.at[chip], mix_all.at[chip])
     drain(2 * len(order))
     forward(pack_spread, pack_recv, pack_twins, pack_pushes)
     settle(pack_twins, pack_recv, pack_pushes)
@@ -512,7 +510,7 @@
         ]
         turned = jnp.concatenate(
             [
-                jnp.concatenate([pack_recv[2 * source + j, i, :hidden, :] for i in range(2)], axis=0)
+                jnp.concatenate([pack_recv[source, j, i, :hidden, :] for i in range(2)], axis=0)
                 for j in range(2)
             ],
             axis=1,
@@ -545,7 +543,7 @@
     ]
     shared_rows = jnp.concatenate(
         [
-            jnp.concatenate([pack_recv[i, j, hidden:, :] for i in range(n)], axis=1)
+            jnp.concatenate([pack_recv[i // 2, i % 2, j, hidden:, :] for i in range(n)], axis=1)
             for j in range(2)
         ],
         axis=0,
@@ -574,7 +572,7 @@
         part_send[i] = value.astype(BF16)
         fifth.append(
             spread(
-                (8, 9)[i], lambda there: part_send.at[i, there], sum_recv.at[i, chip]
+                (0, 2)[i], lambda there: part_send.at[i, there], sum_recv.at[i, chip]
             )
         )
     drain(2 * len(order))
@@ -652,7 +650,7 @@
             VMEM((rows, top_count), F32),
             VMEM(shared_gate.shape, BF16),
             VMEM(shared_up.shape, BF16),
-            VMEM((chips, 2, cut // 2, width // chips), BF16),
+            VMEM(out_weight.shape, BF16),
             VMEM((4, 2, cut, width), BF16),
             VMEM((2, 2, width, inner), BF16),
             VMEM((2, inner, width), BF16),
@@ -662,24 +660,24 @@
             VMEM((chips, rows, 8 * cut), BF16),
             VMEM((chips, rows, 8 * cut), BF16),
             VMEM((chips, rows, heads * size), BF16),
-            VMEM((n, 2, cut // 2, width // chips), BF16),
+            VMEM((chips, 2, 2, cut // 2, width // chips), BF16),
             VMEM((chips, chips * rows, width // chips), BF16),
             VMEM((chips, rows, width), F32),
             VMEM((chips, 2, 3 * hidden // 2, lean), BF16),
-            VMEM((n, 2, 3 * hidden // 2, lean), BF16),
+            VMEM((chips, 2, 2, 3 * hidden // 2, lean), BF16),
             VMEM((2, chips, rows, width // 2), F32),
             VMEM((2, chips, rows, width // 2), BF16),
             VMEM((2, chips, rows, width // 2), BF16),
             VMEM((chips, 1, width // chips), F32),
             VMEM((chips * rows, 4 * inner + 128), F32),
-            dma((24 + 2 * chips,)),
-            dma((heads,)),
-            dma((10, chips)),
-            dma((10, chips)),
-            dma((10 + 4 * chips,)),
-            dma((10 + 4 * chips,)),
-            dma((2 * chips,)),
-            dma((2 * chips,)),
+            dma((24,)),
+            dma((4,)),
+            dma((5, chips - 1)),
+            dma((5, chips - 1)),
+            dma((11,)),
+            dma((11,)),
+            dma((2,)),
+            dma((2,)),
         ],
         compiler_params=pltpu.CompilerParams(
             collective_id=0, has_side_effects=True, vmem_limit_bytes=36 * 1024 * 1024

time: 46.9 us -> 45.5 us (0.970)
  Pallas kernels: 46.1 us -> 44.7 us
    pallas_call x1, Pallas kernels: 44 us -> 42.6 us  [fused_shards(): pl.pallas_call(functools.partial(fused, n), out_shape=results, in_specs=[...]
where the time goes in v4:
time: 45.5 us; the launch traced here: 45.4 us
  Pallas kernels  44.7 us (98%)
  between operations  0.65 us (1%)
    pallas_call x1, Pallas kernels, fused_shards(): pl.pallas_call(functools.partial(fused, n), out_shape=results, in_specs=[...  42.6 us
    pallas_call x1, Pallas kernels, fused_shards(): pl.pallas_call(flush, out_shape=results, in_specs=[pl.BlockSpec(memory_sp...  2.11 us

profile of v4, /device:TPU:0, one launch (start us, length us, event | category | flops | bytes accessed | tf_op | source)
XLA Modules:
  0.0 45.4 jit_solution(7943435039602533479)
XLA Ops:
  0.6 42.6 %shard_map.255 = (bf16[8,2048]{1,0:T(8,128)(2,1)S(1)}, f32[8,8,128,128]{3,2,1,0:T(8,128)S(1)}, f32[8,8,128]{2,1,0:T(8,128)S(1)}, f32[8,8]{1,0:T(8,128)S(1)}) custom-call(bf16[8,2048]{1,0:T(8,128)(2,1)} %refs_0_.1, bf16[16,128]{1,0:T(8,128)(2,1)} %bitcast.19, bf16[64,2048]{1,0:T(8,128)(2,1)} %bitcast.12, bf16[64,2048]{1,0:T(8,128)(2,1)} %bitcast.13, ...), custom_call_target="tpu_custom_call" | custom-call | tf_op jit(solution)/shard_map/pallas_call | solution.py:636
  43.3 2.1 %shard_map.256 = (bf16[8,2048]{1,0:T(8,128)(2,1)}, f32[8,8,128,128]{3,2,1,0:T(8,128)}, f32[8,8,128]{2,1,0:T(8,128)}, f32[8,8]{1,0:T(8,128)}) custom-call(bf16[8,2048]{1,0:T(8,128)(2,1)S(1)} %get-tuple-element.8.refs_0_, f32[8,8,128,128]{3,2,1,0:T(8,128)S(1)} %get-tuple-element.9.refs_1_, f32[8,8,128]{2,1,0:T(8,128)S(1)} %get-tuple-element.10.refs_2_, ...), custom_call_target="tpu_custom_call" | custom-call | tf_op jit(solution)/shard_map/pallas_call | solution.py:686
